TPU v7x, 512 devices: a 8x2x16 block of a 8x8x16 slice. The times are simulated.
512 devices in a mesh: grp: 2 (over y), sp: 32 (over z, core), tp: 8 (over x).
Axes of the slice: x: 8, y: 2, z: 16, core: 2. Of those that a mesh axis runs over, the one named last changes fastest.
The devices are a block of a 8x8x16 slice.
Arguments:
- glu_value: bfloat16 [8192, 2048], P(('grp', 'sp'), 'tp'), parts along dimension 0, may hold values from -6 to 6
- glu_gate: bfloat16 [8192, 2048], P(('grp', 'sp'), 'tp'), parts along dimension 0, may hold values from -9 to 9
- segments: int32 [8192], P(('grp', 'sp')), parts along dimension 0, may hold values from 0 to 7, never falling along the last dimension, each value on 1 to 2048 neighbouring positions
- conv_kernel: float32 [31, 2048], P(None, 'tp'), may hold values from -3.5 to 3.5
- norm_gain: float32 [2048], P('tp'), may hold values from 0.1 to 1.9
- norm_bias: float32 [2048], P('tp'), may hold values from -3 to 3
- residual: bfloat16 [8192, 2048], P(('grp', 'sp'), 'tp'), parts along dimension 0, may hold values from -6 to 6
- out_weight: bfloat16 [2048, 2048], P('tp'), may hold values from -0.125 to 0.125
- rms_gain: float32 [2048], replicated, may hold values from 0.1 to 1.9
- experts: int32 [8192, 4], P(('grp', 'sp')), parts along dimension 0, may hold values from 0 to 31, all different within a row; in each aligned block of 128 rows (0 to 127, 128 to 255, ...) at most 32 rows name the same one
- route_weights: float32 [8192, 4], P(('grp', 'sp')), parts along dimension 0, may hold values from 0.1 to 1
- glu_weight: bfloat16 [32, 2048, 2048], P('sp', None, 'tp'), may hold values from -0.5 to 0.5
- lin_weight: bfloat16 [32, 2048, 2048], P('sp', None, 'tp'), may hold values from -0.5 to 0.5
- down_weight: bfloat16 [32, 2048, 2048], P('sp', None, 'tp'), may hold values from -0.015625 to 0.015625
Outputs:
- layer_output: bfloat16 [8192, 2048], P(('grp', 'sp'), 'tp'), parts along dimension 0
There are 2 independent parts, one for each index of `grp`. A program takes and returns all parts, laid end to end along the dimension named above; an argument that names none is the same for every part. Nothing has to cross between parts.
Inputs may be any that keep to these rules, and one draw needn't show every extreme that they name: Each row names 4 different experts. In each aligned block of 128 rows no expert is named by more than 32 rows, and in some block an expert is named by exactly 32 rows. `segments`: never falling along positions; a document holds from 1 up to 2048 positions, and one holds exactly that many.
All inputs are finite; a program needn't handle non-finite values.
Results may differ from a plain program's by a relative error of at most 0.017.
Values may be sent and summed in bfloat16 or wider, within the bound.
No kernel may reach another device: no remote copies, remote signals or barrier semaphores. Data moves between devices by JAX's collectives and lax.ppermute only.
A program may use at most 64 MiB of HBM per device.

v0:
```python
import jax
import jax.numpy as jnp
from jax import lax
from jax.sharding import PartitionSpec as P

EPSILON = 1e-05
CLAMP_LIMIT = 7.0
SIGMOID_SCALE = 1.702


def passed_along(array, axis, by):
    length = lax.axis_size(axis)
    pairs = [(i, i + by) for i in range(length) if 0 <= i + by < length]
    return lax.ppermute(array, axis, pairs)


def copy_for_each(array, axis):
    copies = jnp.broadcast_to(array, (lax.axis_size(axis), *array.shape))
    return lax.all_to_all(copies, axis, split_axis=0, concat_axis=0, tiled=True)


def of_everyone(array, axis):
    return copy_for_each(array, axis).sum(axis=0)


def in_one(arrays, axis):
    ends = [0]
    for a in arrays:
        ends.append(ends[-1] + a.size)
    total = of_everyone(jnp.concatenate([a.ravel() for a in arrays]), axis)
    return tuple((total[b:e].reshape(a.shape) for a, b, e in zip(arrays, ends, ends[1:])))


def in_blocks(array, dim, length):
    lengths = array.shape
    blocks = array.reshape(*lengths[:dim], length, lengths[dim] // length, *lengths[dim + 1 :])
    return jnp.moveaxis(blocks, dim, 0)


def summed_on_arrival(array, axis, dim):
    length = lax.axis_size(axis)
    blocks = lax.all_to_all(in_blocks(array, dim, length), axis, 0, 0, tiled=True)
    return jnp.sum(blocks.astype(jnp.float32), axis=0)


def clamped_unit(gate_pre, lin_pre):
    gate_clip = jnp.minimum(gate_pre, CLAMP_LIMIT)
    linear = jnp.clip(lin_pre, -CLAMP_LIMIT, CLAMP_LIMIT)
    return gate_clip * jax.nn.sigmoid(SIGMOID_SCALE * gate_clip) * (linear + 1.0)


def shards(
    glu_value,
    glu_gate,
    segments,
    conv_kernel,
    norm_gain,
    norm_bias,
    residual,
    out_weight,
    rms_gain,
    experts,
    route_weights,
    glu_weight,
    lin_weight,
    down_weight,
):
    tok_count = glu_value.shape[0]
    local_width = glu_value.shape[1]
    model_width = out_weight.shape[1]
    kernel_reach = conv_kernel.shape[0] - 1
    top_count = experts.shape[1]
    local_experts = glu_weight.shape[0]
    sp_count = lax.axis_size("sp")
    expert_total = local_experts * sp_count
    capacity = min(tok_count, 2 * tok_count * top_count // expert_total)
    glu_out = (glu_value.astype(jnp.float32) * jax.nn.sigmoid(glu_gate.astype(jnp.float32))).astype(
        jnp.bfloat16
    )
    prev_rows, prev_segments = passed_along(
        (glu_out[tok_count - kernel_reach :], segments[tok_count - kernel_reach :]), "sp", 1
    )
    padded = jnp.concatenate([prev_rows, glu_out], axis=0).astype(jnp.float32)
    padded_segments = jnp.concatenate([prev_segments, segments], axis=0)
    conv_sum = jnp.zeros((tok_count, local_width), jnp.float32)
    for offset in range(kernel_reach + 1):
        lower = kernel_reach - offset
        window_rows = padded[lower : lower + tok_count]
        same_document = (padded_segments[lower : lower + tok_count] == segments).astype(jnp.float32)
        conv_sum = conv_sum + conv_kernel[offset][None, :] * window_rows * same_document[:, None]
    row_total, row_square = in_one(
        (jnp.sum(conv_sum, axis=1), jnp.sum(conv_sum * conv_sum, axis=1)), "tp"
    )
    row_mean = row_total / model_width
    row_var = row_square / model_width - row_mean * row_mean
    normed_conv = (conv_sum - row_mean[:, None]) * lax.rsqrt(row_var + EPSILON)[
        :, None
    ] * norm_gain + norm_bias
    swished = jax.nn.silu(normed_conv).astype(jnp.bfloat16)
    projected = jnp.dot(swished, out_weight, preferred_element_type=jnp.float32)
    conv_out = summed_on_arrival(projected.astype(jnp.bfloat16), "tp", 1)
    updated = (residual.astype(jnp.float32) + conv_out).astype(jnp.bfloat16)
    updated_float = updated.astype(jnp.float32)
    flat_experts = experts.reshape(-1)
    one_hot = (flat_experts[:, None] == jnp.arange(expert_total, dtype=jnp.int32)[None, :]).astype(
        jnp.int32
    )
    slot_rank = jnp.sum((jnp.cumsum(one_hot, axis=0) - 1) * one_hot, axis=1)
    slot_index = flat_experts * capacity + slot_rank
    token_order = jnp.arange(tok_count * top_count, dtype=jnp.int32) // top_count
    slot_token = (
        jnp.full((expert_total * capacity,), tok_count, jnp.int32).at[slot_index].set(token_order)
    )
    squares = of_everyone(jnp.sum(updated_float * updated_float, axis=1), "tp")
    width_start = lax.axis_index("tp") * local_width
    gain_cols = lax.dynamic_slice_in_dim(rms_gain, width_start, local_width)
    normed = (
        updated_float * lax.rsqrt(squares / model_width + EPSILON)[:, None] * gain_cols
    ).astype(jnp.bfloat16)
    normed_pad = jnp.concatenate([normed, jnp.zeros((1, local_width), jnp.bfloat16)], axis=0)
    packed = normed_pad[slot_token].reshape(sp_count, local_experts, capacity, local_width)
    portion = lax.all_gather(
        lax.all_to_all(packed, "sp", split_axis=0, concat_axis=0, tiled=True),
        "tp",
        axis=3,
        tiled=True,
    )
    gate_pre = jnp.einsum("slmd,ldf->slmf", portion, glu_weight, preferred_element_type=jnp.float32)
    lin_pre = jnp.einsum("slmd,ldf->slmf", portion, lin_weight, preferred_element_type=jnp.float32)
    hidden = clamped_unit(gate_pre, lin_pre).astype(jnp.bfloat16)
    summed = jnp.einsum(
        "slmf,lfd->slmd",
        lax.all_gather(hidden, "tp", axis=3, tiled=True),
        down_weight,
        preferred_element_type=jnp.float32,
    )
    results = summed.astype(jnp.bfloat16)
    returned = lax.all_to_all(results, "sp", split_axis=0, concat_axis=0, tiled=True)
    flat_back = returned.reshape(expert_total * capacity, local_width)
    picked = flat_back[slot_index].reshape(tok_count, top_count, local_width).astype(jnp.float32)
    routed_sum = jnp.sum(picked * route_weights[:, :, None], axis=1)
    return (updated_float + routed_sum).astype(jnp.bfloat16)


def solution(mesh):
    in_specs = (
        P(("grp", "sp"), "tp"),
        P(("grp", "sp"), "tp"),
        P(("grp", "sp")),
        P(None, "tp"),
        P("tp"),
        P("tp"),
        P(("grp", "sp"), "tp"),
        P("tp", None),
        P(),
        P(("grp", "sp"), None),
        P(("grp", "sp"), None),
        P("sp", None, "tp"),
        P("sp", None, "tp"),
        P("sp", None, "tp"),
    )
    out_specs = P(("grp", "sp"), "tp")
    return jax.shard_map(shards, mesh=mesh, in_specs=in_specs, out_specs=out_specs, check_vma=False)
```

profile of v0, /device:TPU:65, one launch (start us, length us, event | category | flops | bytes accessed | tf_op | source)
XLA Modules:
  0.0 342.0 jit_solution(18076324857074876872)
XLA Ops:
  7.4 7.0 %collective-permute-start.1 = (s32[30]{0:T(128)S(1)}, s32[30]{0:T(128)S(1)}, u32[]{:S(2)}, u32[]{:S(2)}) collective-permute-start(s32[30]{0:T(128)S(1)} %slice.299), channel_id=1, source_target_pairs={{0,8},{8,16},{16,24},{24,32},{32,40},{40,48},{48,56},{56,64},{64,7... | collective-permute-start | bytes 368 | tf_op jit(solution)/shard_map/ppermute | solution.py:14
  15.4 2.0 collective-permute-start
  17.3 1.0 fusion.117
  18.4 1.0 fusion.118
  19.3 31.4 %collective-permute-done.1 = s32[30]{0:T(128)S(1)} collective-permute-done((s32[30]{0:T(128)S(1)}, s32[30]{0:T(128)S(1)}, u32[]{:S(2)}, u32[]{:S(2)}) %collective-permute-start.1) | collective-permute-done | bytes 152 | tf_op jit(solution)/shard_map/ppermute | solution.py:14
  53.1 0.9 fusion.115
  54.6 3.5 %all-to-all-start = ((f32[8,1,256]{2,1,0:T(1,128)}), f32[8,1,256]{2,1,0:T(1,128)S(1)}, u32[]{:S(2)}, u32[]{:S(2)}) async-start(f32[8,1,256]{2,1,0:T(1,128)} %broadcast_in_dim.8), calls=%async_computation | async-start | bytes 16384 | tf_op jit(solution)/shard_map/all_to_all | solution.py:19
  58.5 6.0 %all-to-all-done = f32[8,1,256]{2,1,0:T(1,128)S(1)} async-done(((f32[8,1,256]{2,1,0:T(1,128)}), f32[8,1,256]{2,1,0:T(1,128)S(1)}, u32[]{:S(2)}, u32[]{:S(2)}) %all-to-all-start) | async-done | bytes 8224 | tf_op jit(solution)/shard_map/all_to_all | solution.py:19
  65.8 3.7 %all-to-all-start.1 = ((bf16[8,128,256]{2,1,0:T(8,128)(2,1)}), bf16[8,128,256]{2,1,0:T(8,128)(2,1)S(1)}, u32[]{:S(2)}, u32[]{:S(2)}) async-start(bf16[8,128,256]{2,1,0:T(8,128)(2,1)} %bitcast.123), calls=%async_computation.1 | async-start | bytes 1048576 | tf_op jit(solution)/shard_map/all_to_all | solution.py:42
  69.5 1.2 reduce-window.6
  71.3 2.4 scatter_custom_fusion
  73.8 7.1 %all-to-all-done.1 = bf16[8,128,256]{2,1,0:T(8,128)(2,1)S(1)} async-done(((bf16[8,128,256]{2,1,0:T(8,128)(2,1)}), bf16[8,128,256]{2,1,0:T(8,128)(2,1)S(1)}, u32[]{:S(2)}, u32[]{:S(2)}) %all-to-all-start.1) | async-done | bytes 524320 | tf_op jit(solution)/shard_map/all_to_all | solution.py:42
  81.7 4.3 %all-to-all-start.2 = ((f32[8,1,128]{2,1,0:T(1,128)}), f32[8,1,128]{2,1,0:T(1,128)S(1)}, u32[]{:S(2)}, u32[]{:S(2)}) async-start(f32[8,1,128]{2,1,0:T(1,128)} %broadcast_in_dim.9), calls=%async_computation.2 | async-start | bytes 8192 | tf_op jit(solution)/shard_map/all_to_all | solution.py:19
  86.8 5.6 %all-to-all-done.2 = f32[8,1,128]{2,1,0:T(1,128)S(1)} async-done(((f32[8,1,128]{2,1,0:T(1,128)}), f32[8,1,128]{2,1,0:T(1,128)S(1)}, u32[]{:S(2)}, u32[]{:S(2)}) %all-to-all-start.2) | async-done | bytes 4128 | tf_op jit(solution)/shard_map/all_to_all | solution.py:19
  92.6 3.9 %gather_fusion = bf16[1024,256]{1,0:T(8,128)(2,1)S(1)} fusion(bf16[129,256]{1,0:T(8,128)(2,1)S(1)} %concatenate.15, s32[1024]{0:T(1024)S(1)} %fusion.108), kind=kCustom, calls=%fused_computation | custom fusion | bytes 1052672 | tf_op jit(solution)/shard_map/gather | solution.py:121
  96.5 53.6 %all_to_all.27 = bf16[32,1,32,256]{3,2,1,0:T(8,128)(2,1)} all-to-all(bf16[32,1,32,256]{3,2,1,0:T(8,128)(2,1)S(1)} %bitcast.127), channel_id=1, replica_groups=mesh['grp'=2,'sp'=32,'tp'=8] {'sp'}, dimensions={0} | all-to-all | bytes 1048576 | tf_op jit(solution)/shard_map/all_to_all | solution.py:123
  150.2 54.3 %all-gather.3.cloned.1.call-done = bf16[32,1,32,2048]{3,2,0,1:T(8,128)(2,1)} async-done(((bf16[32,1,32,256]{3,2,0,1:T(8,128)(2,1)}), bf16[32,1,32,2048]{3,2,0,1:T(8,128)(2,1)}) %all-gather.3.cloned.1.call-update) | async-done | bytes 4194320 | tf_op jit(solution)/shard_map/all_gather | solution.py:122
  204.5 3.6 %fusion.9 = f32[32,1,32,256]{3,2,0,1:T(8,128)S(1)} fusion(bf16[32,1,32,2048]{3,2,0,1:T(8,128)(2,1)} %all-gather.3.cloned.1.call-done, bf16[1,2048,256]{2,1,0:T(8,128)(2,1)S(1)} %copy-done.7), kind=kOutput, calls=%fused_computation.11 | convolution fusion | flops 1074003968 | bytes 6291456 | tf_op jit(solution)/shard_map/slmd,ldf->slmf/dot_general | solution.py:128
  208.1 3.5 %fusion.24 = bf16[32,1,32,256]{3,2,0,1:T(8,128)(2,1)} fusion(bf16[32,1,32,2048]{3,2,0,1:T(8,128)(2,1)S(1)} %copy-done.6, bf16[1,2048,256]{2,1,0:T(8,128)(2,1)} %param.26, f32[32,1,32,256]{3,2,0,1:T(8,128)S(1)} %fusion.9), kind=kOutput, calls=%fused_computation.16 | convolution fusion | flops 1076101120 | bytes 6815744 | tf_op jit(solution)/shard_map/slmd,ldf->slmf/dot_general | solution.py:129
  211.7 67.7 %all-gather.5.cloned.1.call-done = bf16[32,1,32,2048]{3,2,0,1:T(8,128)(2,1)} async-done(((bf16[32,1,32,256]{3,2,0,1:T(8,128)(2,1)}), bf16[32,1,32,2048]{3,2,0,1:T(8,128)(2,1)}) %all-gather.5.cloned.1.call-update) | async-done | bytes 4194320 | tf_op jit(solution)/shard_map/all_gather | solution.py:133
  279.4 4.2 %fusion.30 = bf16[32,1,32,256]{3,2,1,0:T(8,128)(2,1)} fusion(bf16[32,1,32,2048]{3,2,0,1:T(8,128)(2,1)} %all-gather.5.cloned.1.call-done, bf16[1,2048,256]{2,1,0:T(8,128)(2,1)S(1)} %copy-done.8), kind=kOutput, calls=%fused_computation.18 | convolution fusion | flops 1074003968 | bytes 5767168 | tf_op jit(solution)/shard_map/slmf,lfd->slmd/dot_general | solution.py:131
  283.6 15.1 %all-to-all-start.4 = ((bf16[32,1,32,256]{3,2,1,0:T(8,128)(2,1)}), bf16[32,1,32,256]{3,2,1,0:T(8,128)(2,1)S(1)}, u32[]{:S(2)}, u32[]{:S(2)}) async-start(bf16[32,1,32,256]{3,2,1,0:T(8,128)(2,1)} %fusion.30), calls=%async_computation.4 | async-start | bytes 1048576 | tf_op jit(solution)/shard_map/all_to_all | solution.py:138
  298.8 33.2 %all-to-all-done.4 = bf16[32,1,32,256]{3,2,1,0:T(8,128)(2,1)S(1)} async-done(((bf16[32,1,32,256]{3,2,1,0:T(8,128)(2,1)}), bf16[32,1,32,256]{3,2,1,0:T(8,128)(2,1)S(1)}, u32[]{:S(2)}, u32[]{:S(2)}) %all-to-all-start.4) | async-done | bytes 524320 | tf_op jit(solution)/shard_map/all_to_all | solution.py:138
  332.0 1.9 gather_fusion.1
  (63 shorter events, 10.1 us)
Async XLA Ops:
  6.5 58.0 %copy-start = (bf16[256,2048]{1,0:T(8,128)(2,1)S(1)}, bf16[256,2048]{1,0:T(8,128)(2,1)}, u32[]{:S(2)}) copy-start(bf16[256,2048]{1,0:T(8,128)(2,1)} %param.21) | copy-start | bytes 3145732
  6.6 51.6 %copy-start.2 = (s32[128,4]{0,1:T(4,128)S(1)}, s32[128,4]{0,1:T(4,128)}, u32[]{:S(2)}) copy-start(s32[128,4]{0,1:T(4,128)} %param.23) | copy-start | bytes 6148
  6.6 58.0 %copy-start.5 = (f32[256]{0:T(256)S(1)}, f32[256]{0:T(256)}, u32[]{:S(2)}) copy-start(f32[256]{0:T(256)} %param.18) | copy-start | bytes 3076
  6.6 58.0 %copy-start.4 = (f32[256]{0:T(256)S(1)}, f32[256]{0:T(256)}, u32[]{:S(2)}) copy-start(f32[256]{0:T(256)} %param.19) | copy-start | bytes 3076
  7.4 43.4 %collective-permute-start.1 = (s32[30]{0:T(128)S(1)}, s32[30]{0:T(128)S(1)}, u32[]{:S(2)}, u32[]{:S(2)}) collective-permute-start(s32[30]{0:T(128)S(1)} %slice.299), channel_id=1, source_target_pairs={{0,8},{8,16},{16,24},{24,32},{32,40},{40,48},{48,56},{56,64},{64,7... | collective-permute-start | bytes 368 | tf_op jit(solution)/shard_map/ppermute | solution.py:14
  15.4 37.6 %collective-permute-start = (bf16[30,256]{1,0:T(8,128)(2,1)S(1)}, bf16[30,256]{1,0:T(8,128)(2,1)S(1)}, u32[]{:S(2)}, u32[]{:S(2)}) collective-permute-start(bf16[30,256]{1,0:T(8,128)(2,1)S(1)} %slice.396), channel_id=1, source_target_pairs={{0,8},{8,16},{16,24},{24,32},{32,40},{40,48},{48,56},{56,64},{64,7... | collective-permute-start | bytes 46088 | tf_op jit(solution)/shard_map/ppermute | solution.py:14
  53.0 27.9 %copy-start.1 = (bf16[128,256]{1,0:T(8,128)(2,1)S(1)}, bf16[128,256]{1,0:T(8,128)(2,1)}, u32[]{:S(2)}) copy-start(bf16[128,256]{1,0:T(8,128)(2,1)} %param.20) | copy-start | bytes 196612
  54.6 9.9 %all-to-all-start = ((f32[8,1,256]{2,1,0:T(1,128)}), f32[8,1,256]{2,1,0:T(1,128)S(1)}, u32[]{:S(2)}, u32[]{:S(2)}) async-start(f32[8,1,256]{2,1,0:T(1,128)} %broadcast_in_dim.8), calls=%async_computation | async-start | bytes 16384 | tf_op jit(solution)/shard_map/all_to_all | solution.py:19
  65.8 15.1 %all-to-all-start.1 = ((bf16[8,128,256]{2,1,0:T(8,128)(2,1)}), bf16[8,128,256]{2,1,0:T(8,128)(2,1)S(1)}, u32[]{:S(2)}, u32[]{:S(2)}) async-start(bf16[8,128,256]{2,1,0:T(8,128)(2,1)} %bitcast.123), calls=%async_computation.1 | async-start | bytes 1048576 | tf_op jit(solution)/shard_map/all_to_all | solution.py:42
  69.5 135.0 %copy-start.7 = (bf16[1,2048,256]{2,1,0:T(8,128)(2,1)S(1)}, bf16[1,2048,256]{2,1,0:T(8,128)(2,1)}, u32[]{:S(2)}) copy-start(bf16[1,2048,256]{2,1,0:T(8,128)(2,1)} %param.25) | copy-start | bytes 3145732
  81.7 10.8 %all-to-all-start.2 = ((f32[8,1,128]{2,1,0:T(1,128)}), f32[8,1,128]{2,1,0:T(1,128)S(1)}, u32[]{:S(2)}, u32[]{:S(2)}) async-start(f32[8,1,128]{2,1,0:T(1,128)} %broadcast_in_dim.9), calls=%async_computation.2 | async-start | bytes 8192 | tf_op jit(solution)/shard_map/all_to_all | solution.py:19
  86.0 118.6 %all-gather.3.cloned.1.call-start = ((), (), s32[]{:S(2)}) async-start(), calls=%async_computation.5 | async-start | bytes 4718592 | tf_op jit(solution)/shard_map/all_gather | solution.py:122
  150.2 129.2 %all-gather.5.cloned.1.call-start = ((), (), s32[]{:S(2)}) async-start(), calls=%async_computation.6 | async-start | bytes 4718592 | tf_op jit(solution)/shard_map/all_gather | solution.py:133
  204.5 3.6 %copy-start.6 = (bf16[32,1,32,2048]{3,2,0,1:T(8,128)(2,1)S(1)}, bf16[32,1,32,2048]{3,2,0,1:T(8,128)(2,1)}, u32[]{:S(2)}) copy-start(bf16[32,1,32,2048]{3,2,0,1:T(8,128)(2,1)} %all-gather.3.cloned.1.call-done) | copy-start | bytes 12582916
  208.1 71.2 %copy-start.8 = (bf16[1,2048,256]{2,1,0:T(8,128)(2,1)S(1)}, bf16[1,2048,256]{2,1,0:T(8,128)(2,1)}, u32[]{:S(2)}) copy-start(bf16[1,2048,256]{2,1,0:T(8,128)(2,1)} %param.27) | copy-start | bytes 3145732
  211.7 87.0 %copy-start.3 = (f32[128,4]{0,1:T(4,128)S(1)}, f32[128,4]{0,1:T(4,128)}, u32[]{:S(2)}) copy-start(f32[128,4]{0,1:T(4,128)} %param.24) | copy-start | bytes 6148
  283.6 48.4 %all-to-all-start.4 = ((bf16[32,1,32,256]{3,2,1,0:T(8,128)(2,1)}), bf16[32,1,32,256]{3,2,1,0:T(8,128)(2,1)S(1)}, u32[]{:S(2)}, u32[]{:S(2)}) async-start(bf16[32,1,32,256]{3,2,1,0:T(8,128)(2,1)} %fusion.30), calls=%async_computation.4 | async-start | bytes 1048576 | tf_op jit(solution)/shard_map/all_to_all | solution.py:138
Sparse Core Ops, SparseCore 0:
  150.3 54.1 all-gather.2
  211.8 67.5 all-gather.4
where the time goes:
time: 343 us; the launch traced here: 342 us
  waiting for transfers between devices  205 us (60%)
  blocking collectives  53.6 us (16%)
  starting transfers between devices  35.7 us (10%)
  local copies, waits for them, and re-layouts  15 us (4%)
  between operations  13.7 us (4%)
  matrix products  11.7 us (3%)
  other arithmetic  6.8 us (2%)
    all_gather x1, waiting for transfers between devices, shards(): lax.all_gather(hidden, 'tp', axis=3, tiled=True)  67.7 us
    all_gather x1, waiting for transfers between devices, shards(): lax.all_gather(lax.all_to_all(packed, 'sp', split_axis=0, concat_axis=0,...  54.3 us
    all_to_all x1, blocking collectives, shards(): lax.all_to_all(packed, 'sp', split_axis=0, concat_axis=0, tiled=True)  53.6 us
    all_to_all x1, waiting for transfers between devices, shards(): lax.all_to_all(results, 'sp', split_axis=0, concat_axis=0, tiled=True)  33.2 us
    ppermute x2, waiting for transfers between devices, passed_along(): return lax.ppermute(array, axis, pairs)  31.5 us
    all_to_all x1, starting transfers between devices, shards(): lax.all_to_all(results, 'sp', split_axis=0, concat_axis=0, tiled=True)  15.1 us
    all_to_all x2, waiting for transfers between devices, copy_for_each(): return lax.all_to_all(copies, axis, split_axis=0, concat_axis=0, tiled=True)  11.7 us
    ppermute x2, starting transfers between devices, passed_along(): return lax.ppermute(array, axis, pairs)  9 us
  transfers between devices with their start and end apart: 8, of which 7 were waited for; matrix products, arithmetic and copies ran while one was open for 3% of the time, Pallas kernels for 0%

commit v1 on v0

--- a/solution.py
+++ b/solution.py
@@ -6,6 +6,11 @@
 EPSILON = 1e-05
 CLAMP_LIMIT = 7.0
 SIGMOID_SCALE = 1.702
+
+
+def tiled_gather(value, axis, dim):
+    copies = jnp.concatenate([value] * lax.axis_size(axis), axis=dim)
+    return lax.all_to_all(copies, axis, dim, dim, tiled=True)
 
 
 def passed_along(array, axis, by):
@@ -130,7 +135,7 @@
     hidden = clamped_unit(gate_pre, lin_pre).astype(jnp.bfloat16)
     summed = jnp.einsum(
         "slmf,lfd->slmd",
-        lax.all_gather(hidden, "tp", axis=3, tiled=True),
+        tiled_gather(hidden, "tp", 3),
         down_weight,
         preferred_element_type=jnp.float32,
     )

time: 343 us -> 449 us (1.31)
  blocking collectives: 53.6 us -> 149 us
  local copies, waits for them, and re-layouts: 15 us -> 92.9 us
  waiting for transfers between devices: 205 us -> 138 us
    all_to_all x0 -> x1, blocking collectives: none -> 95 us  [tiled_gather(): return lax.all_to_all(copies, axis, dim, dim, tiled=True)]
    all_gather x1 -> x0, waiting for transfers between devices: 67.7 us -> none  [shards(): lax.all_gather(hidden, 'tp', axis=3, tiled=True)]
    unnamed x20 -> x30, local copies, waits for them, and re-layouts: 0.27 us -> 36.6 us
    concatenate x0 -> x2, local copies, waits for them, and re-layouts: none -> 23.9 us  [tiled_gather(): copies = jnp.concatenate([value] * lax.axis_size(axis), axis=dim)]
    all_to_all x0 -> x1, local copies, waits for them, and re-layouts: none -> 17.6 us  [tiled_gather(): return lax.all_to_all(copies, axis, dim, dim, tiled=True)]
  transfers between devices with their start and end apart: 8 -> 7, of which waited for: 7 -> 6; matrix products, arithmetic and copies ran while one was open for 3% -> 2% of each run, Pallas kernels for 0% -> 0%
where the time goes in v1:
time: 449 us; the launch traced here: 448 us
  blocking collectives  149 us (33%)
  waiting for transfers between devices  138 us (31%)
  local copies, waits for them, and re-layouts  92.9 us (21%)
  starting transfers between devices  37.5 us (8%)
  between operations  13.7 us (3%)
  matrix products  10.5 us (2%)
  other arithmetic  6.8 us (2%)
    all_to_all x1, blocking collectives, tiled_gather(): return lax.all_to_all(copies, axis, dim, dim, tiled=True)  95 us
    all_gather x1, waiting for transfers between devices, shards(): lax.all_gather(lax.all_to_all(packed, 'sp', split_axis=0, concat_axis=0,...  54.4 us
    all_to_all x1, blocking collectives, shards(): lax.all_to_all(packed, 'sp', split_axis=0, concat_axis=0, tiled=True)  53.6 us
    unnamed x30, local copies, waits for them, and re-layouts  36.6 us
    all_to_all x1, waiting for transfers between devices, shards(): lax.all_to_all(results, 'sp', split_axis=0, concat_axis=0, tiled=True)  33.2 us
    ppermute x2, waiting for transfers between devices, passed_along(): return lax.ppermute(array, axis, pairs)  31.5 us
    concatenate x2, local copies, waits for them, and re-layouts, tiled_gather(): copies = jnp.concatenate([value] * lax.axis_size(axis), axis=dim)  23.9 us
    all_to_all x1, local copies, waits for them, and re-layouts, tiled_gather(): return lax.all_to_all(copies, axis, dim, dim, tiled=True)  17.6 us
  transfers between devices with their start and end apart: 7, of which 6 were waited for; matrix products, arithmetic and copies ran while one was open for 2% of the time, Pallas kernels for 0%

profile of v1, /device:TPU:65, one launch (start us, length us, event | category | flops | bytes accessed | tf_op | source)
XLA Modules:
  0.0 447.8 jit_solution(15540208260175600493)
XLA Ops:
  7.4 7.0 %collective-permute-start.1 = (s32[30]{0:T(128)S(1)}, s32[30]{0:T(128)S(1)}, u32[]{:S(2)}, u32[]{:S(2)}) collective-permute-start(s32[30]{0:T(128)S(1)} %slice.299), channel_id=1, source_target_pairs={{0,8},{8,16},{16,24},{24,32},{32,40},{40,48},{48,56},{56,64},{64,7... | collective-permute-start | bytes 368 | tf_op jit(solution)/shard_map/ppermute | solution.py:19
  15.4 2.0 collective-permute-start
  19.4 31.4 %collective-permute-done.1 = s32[30]{0:T(128)S(1)} collective-permute-done((s32[30]{0:T(128)S(1)}, s32[30]{0:T(128)S(1)}, u32[]{:S(2)}, u32[]{:S(2)}) %collective-permute-start.1) | collective-permute-done | bytes 152 | tf_op jit(solution)/shard_map/ppermute | solution.py:19
  54.7 3.5 all-to-all-start
  58.6 6.0 %all-to-all-done = f32[8,1,256]{2,1,0:T(1,128)S(1)} async-done(((f32[8,1,256]{2,1,0:T(1,128)}), f32[8,1,256]{2,1,0:T(1,128)S(1)}, u32[]{:S(2)}, u32[]{:S(2)}) %all-to-all-start) | async-done | bytes 8224 | tf_op jit(solution)/shard_map/all_to_all | solution.py:24
  65.9 3.7 all-to-all-start.1
  71.4 2.4 scatter_custom_fusion
  73.8 7.1 %all-to-all-done.1 = bf16[8,128,256]{2,1,0:T(8,128)(2,1)S(1)} async-done(((bf16[8,128,256]{2,1,0:T(8,128)(2,1)}), bf16[8,128,256]{2,1,0:T(8,128)(2,1)S(1)}, u32[]{:S(2)}, u32[]{:S(2)}) %all-to-all-start.1) | async-done | bytes 524320 | tf_op jit(solution)/shard_map/all_to_all | solution.py:47
  81.7 4.3 all-to-all-start.2
  86.9 5.6 %all-to-all-done.2 = f32[8,1,128]{2,1,0:T(1,128)S(1)} async-done(((f32[8,1,128]{2,1,0:T(1,128)}), f32[8,1,128]{2,1,0:T(1,128)S(1)}, u32[]{:S(2)}, u32[]{:S(2)}) %all-to-all-start.2) | async-done | bytes 4128 | tf_op jit(solution)/shard_map/all_to_all | solution.py:24
  92.6 3.9 gather_fusion
  96.6 53.6 %all_to_all.32 = bf16[32,1,32,256]{3,2,1,0:T(8,128)(2,1)} all-to-all(bf16[32,1,32,256]{3,2,1,0:T(8,128)(2,1)S(1)} %bitcast.135), channel_id=1, replica_groups=mesh['grp'=2,'sp'=32,'tp'=8] {'sp'}, dimensions={0} | all-to-all | bytes 1048576 | tf_op jit(solution)/shard_map/all_to_all | solution.py:128
  150.2 54.4 %all-gather.2.cloned.1.call-done = bf16[32,1,32,2048]{3,2,0,1:T(8,128)(2,1)} async-done(((bf16[32,1,32,256]{3,2,0,1:T(8,128)(2,1)}), bf16[32,1,32,2048]{3,2,0,1:T(8,128)(2,1)}) %all-gather.2.cloned.1.call-update) | async-done | bytes 4194320 | tf_op jit(solution)/shard_map/all_gather | solution.py:127
  204.6 3.6 fusion.9
  208.2 2.3 constant_dynamic-update-slice_fusion.7
  216.6 23.0 %copy.52 = bf16[32,1,32,2048]{2,0,1,3:T(8,128)(2,1)} copy(bf16[32,1,32,2048]{3,2,0,1:T(8,128)(2,1)} %constant_dynamic-update-slice_fusion) | data formatting | bytes 8388608 | tf_op jit(solution)/shard_map/concatenate | solution.py:12
  239.6 18.7 %reshape.177 = bf16[8,2,131072]{2,1,0:T(2,128)(2,1)} reshape(bf16[2048,1,32,32]{3,2,1,0:T(8,128)(2,1)} %bitcast.130) | data formatting | bytes 8388608
  258.3 95.0 %all_to_all.33 = bf16[8,2,131072]{2,1,0:T(2,128)(2,1)} all-to-all(bf16[8,2,131072]{2,1,0:T(2,128)(2,1)} %reshape.177), channel_id=1, replica_groups=mesh['grp'=2,'sp'=32,'tp'=8] {'tp'}, dimensions={0} | all-to-all | bytes 8388608 | tf_op jit(solution)/shard_map/all_to_all | solution.py:13
  353.4 12.4 %reshape.178 = bf16[2048,1,32,32]{3,2,1,0:T(8,128)(2,1)} reshape(bf16[8,2,131072]{2,1,0:T(2,128)(2,1)} %all_to_all.33) | data formatting | bytes 8388608
  365.8 17.6 %copy.53 = bf16[32,1,32,2048]{3,2,0,1:T(8,128)(2,1)} copy(bf16[32,1,32,2048]{2,0,1,3:T(8,128)(2,1)} %bitcast.131) | data formatting | bytes 8388608 | tf_op jit(solution)/shard_map/all_to_all | solution.py:13
  383.4 4.2 fusion.30
  387.6 16.9 %all-to-all-start.5 = ((bf16[32,1,32,256]{3,2,1,0:T(8,128)(2,1)}), bf16[32,1,32,256]{3,2,1,0:T(8,128)(2,1)S(1)}, u32[]{:S(2)}, u32[]{:S(2)}) async-start(bf16[32,1,32,256]{3,2,1,0:T(8,128)(2,1)} %fusion.30), calls=%async_computation.5 | async-start | bytes 1048576 | tf_op jit(solution)/shard_map/all_to_all | solution.py:143
  404.6 33.2 %all-to-all-done.5 = bf16[32,1,32,256]{3,2,1,0:T(8,128)(2,1)S(1)} async-done(((bf16[32,1,32,256]{3,2,1,0:T(8,128)(2,1)}), bf16[32,1,32,256]{3,2,1,0:T(8,128)(2,1)S(1)}, u32[]{:S(2)}, u32[]{:S(2)}) %all-to-all-start.5) | async-done | bytes 524320 | tf_op jit(solution)/shard_map/all_to_all | solution.py:143
  437.8 1.9 gather_fusion.1
  (74 shorter events, 20.2 us)
Async XLA Ops:
  6.5 201.6 %copy-start = (bf16[1,2048,256]{2,1,0:T(8,128)(2,1)S(1)}, bf16[1,2048,256]{2,1,0:T(8,128)(2,1)}, u32[]{:S(2)}) copy-start(bf16[1,2048,256]{2,1,0:T(8,128)(2,1)} %param.26) | copy-start | bytes 3145732
  6.6 51.7 %copy-start.3 = (s32[128,4]{0,1:T(4,128)S(1)}, s32[128,4]{0,1:T(4,128)}, u32[]{:S(2)}) copy-start(s32[128,4]{0,1:T(4,128)} %param.23) | copy-start | bytes 6148
  6.6 58.1 %copy-start.6 = (f32[256]{0:T(256)S(1)}, f32[256]{0:T(256)}, u32[]{:S(2)}) copy-start(f32[256]{0:T(256)} %param.18) | copy-start | bytes 3076
  6.6 58.1 %copy-start.5 = (f32[256]{0:T(256)S(1)}, f32[256]{0:T(256)}, u32[]{:S(2)}) copy-start(f32[256]{0:T(256)} %param.19) | copy-start | bytes 3076
  6.6 58.1 %copy-start.1 = (bf16[256,2048]{1,0:T(8,128)(2,1)S(1)}, bf16[256,2048]{1,0:T(8,128)(2,1)}, u32[]{:S(2)}) copy-start(bf16[256,2048]{1,0:T(8,128)(2,1)} %param.21) | copy-start | bytes 3145732
  7.4 43.4 %collective-permute-start.1 = (s32[30]{0:T(128)S(1)}, s32[30]{0:T(128)S(1)}, u32[]{:S(2)}, u32[]{:S(2)}) collective-permute-start(s32[30]{0:T(128)S(1)} %slice.299), channel_id=1, source_target_pairs={{0,8},{8,16},{16,24},{24,32},{32,40},{40,48},{48,56},{56,64},{64,7... | collective-permute-start | bytes 368 | tf_op jit(solution)/shard_map/ppermute | solution.py:19
  15.4 37.6 %collective-permute-start = (bf16[30,256]{1,0:T(8,128)(2,1)S(1)}, bf16[30,256]{1,0:T(8,128)(2,1)S(1)}, u32[]{:S(2)}, u32[]{:S(2)}) collective-permute-start(bf16[30,256]{1,0:T(8,128)(2,1)S(1)} %slice.396), channel_id=1, source_target_pairs={{0,8},{8,16},{16,24},{24,32},{32,40},{40,48},{48,56},{56,64},{64,7... | collective-permute-start | bytes 46088 | tf_op jit(solution)/shard_map/ppermute | solution.py:19
  53.1 27.9 %copy-start.2 = (bf16[128,256]{1,0:T(8,128)(2,1)S(1)}, bf16[128,256]{1,0:T(8,128)(2,1)}, u32[]{:S(2)}) copy-start(bf16[128,256]{1,0:T(8,128)(2,1)} %param.20) | copy-start | bytes 196612
  54.7 9.9 %all-to-all-start = ((f32[8,1,256]{2,1,0:T(1,128)}), f32[8,1,256]{2,1,0:T(1,128)S(1)}, u32[]{:S(2)}, u32[]{:S(2)}) async-start(f32[8,1,256]{2,1,0:T(1,128)} %broadcast_in_dim.8), calls=%async_computation | async-start | bytes 16384 | tf_op jit(solution)/shard_map/all_to_all | solution.py:24
  65.9 15.1 %all-to-all-start.1 = ((bf16[8,128,256]{2,1,0:T(8,128)(2,1)}), bf16[8,128,256]{2,1,0:T(8,128)(2,1)S(1)}, u32[]{:S(2)}, u32[]{:S(2)}) async-start(bf16[8,128,256]{2,1,0:T(8,128)(2,1)} %bitcast.129), calls=%async_computation.1 | async-start | bytes 1048576 | tf_op jit(solution)/shard_map/all_to_all | solution.py:47
  69.6 135.0 %copy-start.8 = (bf16[1,2048,256]{2,1,0:T(8,128)(2,1)S(1)}, bf16[1,2048,256]{2,1,0:T(8,128)(2,1)}, u32[]{:S(2)}) copy-start(bf16[1,2048,256]{2,1,0:T(8,128)(2,1)} %param.25) | copy-start | bytes 3145732
  81.7 10.8 %all-to-all-start.2 = ((f32[8,1,128]{2,1,0:T(1,128)}), f32[8,1,128]{2,1,0:T(1,128)S(1)}, u32[]{:S(2)}, u32[]{:S(2)}) async-start(f32[8,1,128]{2,1,0:T(1,128)} %broadcast_in_dim.9), calls=%async_computation.2 | async-start | bytes 8192 | tf_op jit(solution)/shard_map/all_to_all | solution.py:24
  86.0 118.6 %all-gather.2.cloned.1.call-start = ((), (), s32[]{:S(2)}) async-start(), calls=%async_computation.6 | async-start | bytes 4718592 | tf_op jit(solution)/shard_map/all_gather | solution.py:127
  204.6 3.6 copy-start.7
  365.8 17.6 %copy-start.9 = (bf16[1,2048,256]{2,1,0:T(8,128)(2,1)S(1)}, bf16[1,2048,256]{2,1,0:T(8,128)(2,1)}, u32[]{:S(2)}) copy-start(bf16[1,2048,256]{2,1,0:T(8,128)(2,1)} %param.27) | copy-start | bytes 3145732
  383.4 21.1 %copy-start.4 = (f32[128,4]{0,1:T(4,128)S(1)}, f32[128,4]{0,1:T(4,128)}, u32[]{:S(2)}) copy-start(f32[128,4]{0,1:T(4,128)} %param.24) | copy-start | bytes 6148
  387.6 50.2 %all-to-all-start.5 = ((bf16[32,1,32,256]{3,2,1,0:T(8,128)(2,1)}), bf16[32,1,32,256]{3,2,1,0:T(8,128)(2,1)S(1)}, u32[]{:S(2)}, u32[]{:S(2)}) async-start(bf16[32,1,32,256]{3,2,1,0:T(8,128)(2,1)} %fusion.30), calls=%async_computation.5 | async-start | bytes 1048576 | tf_op jit(solution)/shard_map/all_to_all | solution.py:143
Sparse Core Ops, SparseCore 0:
  150.4 54.1 all-gather.1
